TPU v7x, 32 devices: a whole 2x2x4 slice. The times are simulated.
32 devices in a mesh: ep: 8 (over z, core), tp: 4 (over y, x).
Axes of the slice: x: 2, y: 2, z: 4, core: 2. Of those that a mesh axis runs over, the one named last changes fastest.
Arguments:
- tokens: bfloat16 [1024, 3072], P('ep', 'tp'), may hold values from -6 to 6
- routes: int32 [1024, 2], P('ep'), may hold values from 0 to 7, all different within a row; in each aligned block of 128 rows (0 to 127, 128 to 255, ...) at most 40 rows name the same one
- gates: float32 [1024, 2], P('ep'), may hold values from 0.1 to 1.5
- cotangent: bfloat16 [1024, 3072], P('ep', 'tp'), may hold values from -6 to 6
- w_gate: bfloat16 [8, 3072, 896], P('ep', 'tp'), may hold values from -0.109375 to 0.109375
- w_up: bfloat16 [8, 3072, 896], P('ep', 'tp'), may hold values from -0.109375 to 0.109375
- w_down: bfloat16 [8, 3072, 896], P('ep', 'tp'), may hold values from -0.1875 to 0.1875
- shared_hidden: bfloat16 [1024, 448], P('ep'), may hold values from -0.2362278 to 0.2362278
Outputs:
- token_grad: bfloat16 [1024, 3072], P('ep', 'tp')
- gate_grad: float32 [1024, 2], P('ep')
- grad_w_gate: float32 [8, 3072, 896], P('ep', 'tp')
- grad_w_up: float32 [8, 3072, 896], P('ep', 'tp')
- grad_w_down: float32 [8, 3072, 896], P('ep', 'tp')
- row_norms: float32 [3, 8, 3072], P(None, 'ep', 'tp')
- grad_shared: float32 [3072, 448], P('tp', 'ep')
- shared_norms: float32 [3072], P('tp')
Inputs may be any that keep to these rules, and one draw needn't show every extreme that they name: `routes`: in each aligned block of 128 rows (the tokens of one index of ep) a row names 2 different experts and no expert is named by more than 40 rows; some expert is named by exactly 40 rows in some blocks.
All inputs are finite; a program needn't handle non-finite values.
Results may differ from a plain program's by a relative error of at most 0.024.
Values may be sent and summed in bfloat16 or wider, within the bound.
A program may use at most 64 MiB of HBM per device.

v0:
```python
import jax
import jax.numpy as jnp
from jax import lax
from jax.sharding import PartitionSpec as P


def slot_targets(routes, experts, capacity):
    chosen = routes.reshape(-1)
    onehot = (chosen[:, None] == jnp.arange(experts, dtype=jnp.int32)[None, :]).astype(jnp.int32)
    earlier = jnp.cumsum(onehot, axis=0) - onehot
    position = jnp.sum(earlier * onehot, axis=1)
    return chosen * capacity + position


def expert_math(gate_sum, up_sum, down_sum):
    sigma = jax.nn.sigmoid(gate_sum)
    active = gate_sum * sigma
    hidden = (active * up_sum).astype(jnp.bfloat16)
    product = jnp.sum(active * up_sum * down_sum, axis=-1).astype(jnp.bfloat16)
    gate_back = (down_sum * up_sum * sigma * (1.0 + gate_sum * (1.0 - sigma))).astype(jnp.bfloat16)
    up_back = (down_sum * active).astype(jnp.bfloat16)
    return (hidden, gate_back, up_back, product)


def on_device(tokens, routes, gates, cotangent, w_gate, w_up, w_down, shared_hidden):
    tok_count, width_part = tokens.shape
    top_count = routes.shape[1]
    local_experts = w_gate.shape[0]
    experts = local_experts * lax.axis_size("ep")
    capacity = 5 * tok_count * top_count // (4 * experts)
    pair_count = tok_count * top_count
    target = slot_targets(routes, experts, capacity)
    source = (
        jnp.zeros((experts * capacity,), jnp.int32)
        .at[target]
        .set(jnp.arange(pair_count, dtype=jnp.int32))
    )
    filled = jnp.zeros((experts * capacity,), jnp.bool_).at[target].set(True)
    scaled = (gates[:, :, None] * cotangent[:, None, :].astype(jnp.float32)).astype(jnp.bfloat16)
    scaled = scaled.reshape(pair_count, width_part)
    zero_row = jnp.zeros((), jnp.bfloat16)
    token_rows = jnp.where(filled[:, None], tokens[source // top_count], zero_row)
    grad_rows = jnp.where(filled[:, None], scaled[source], zero_row)
    token_rows = token_rows.reshape(experts, capacity, width_part)
    grad_rows = grad_rows.reshape(experts, capacity, width_part)
    arrived_tok, arrived_grad = (
        lax.all_to_all(token_rows, "ep", split_axis=0, concat_axis=1, tiled=True),
        lax.all_to_all(grad_rows, "ep", split_axis=0, concat_axis=1, tiled=True),
    )
    gate_part = jnp.einsum("erd,edf->erf", arrived_tok, w_gate, preferred_element_type=jnp.float32)
    up_part = jnp.einsum("erd,edf->erf", arrived_tok, w_up, preferred_element_type=jnp.float32)
    down_part = jnp.einsum("erd,edf->erf", arrived_grad, w_down, preferred_element_type=jnp.float32)
    sums = (
        lax.psum(gate_part.astype(jnp.bfloat16), "tp").astype(jnp.float32),
        lax.psum(up_part.astype(jnp.bfloat16), "tp").astype(jnp.float32),
        lax.psum(down_part.astype(jnp.bfloat16), "tp").astype(jnp.float32),
    )
    hidden, gate_back, up_back, product = expert_math(sums[0], sums[1], sums[2])
    grad_gate = jnp.einsum(
        "erd,erf->edf", arrived_tok, gate_back, preferred_element_type=jnp.float32
    )
    grad_up = jnp.einsum("erd,erf->edf", arrived_tok, up_back, preferred_element_type=jnp.float32)
    grad_down = jnp.einsum("erd,erf->edf", arrived_grad, hidden, preferred_element_type=jnp.float32)
    token_back = jnp.einsum(
        "erf,edf->erd", gate_back, w_gate, preferred_element_type=jnp.float32
    ) + jnp.einsum("erf,edf->erd", up_back, w_up, preferred_element_type=jnp.float32)
    token_back = token_back.astype(jnp.bfloat16)
    back_rows, back_product = (
        lax.all_to_all(token_back, "ep", split_axis=1, concat_axis=0, tiled=True),
        lax.all_to_all(product, "ep", split_axis=1, concat_axis=0, tiled=True),
    )
    per_pair = back_rows.reshape(experts * capacity, width_part)[target]
    per_pair = per_pair.reshape(tok_count, top_count, width_part)
    token_grad = jnp.sum(per_pair.astype(jnp.float32), axis=1).astype(jnp.bfloat16)
    pair_product = back_product.reshape(experts * capacity)[target].reshape(tok_count, top_count)
    gate_grad = pair_product.astype(jnp.float32) / gates
    row_norms = jnp.stack(
        [
            jnp.sum(grad_gate * grad_gate, axis=-1),
            jnp.sum(grad_up * grad_up, axis=-1),
            jnp.sum(grad_down * grad_down, axis=-1),
        ],
        axis=0,
    )
    shared_term = jnp.einsum(
        "td,ts->ds", cotangent, shared_hidden, preferred_element_type=jnp.float32
    )
    grad_shared = lax.psum_scatter(shared_term, "ep", scatter_dimension=1, tiled=True)
    shared_norms = lax.psum(jnp.sum(grad_shared * grad_shared, axis=1), "ep")
    return (
        token_grad,
        gate_grad,
        grad_gate,
        grad_up,
        grad_down,
        row_norms,
        grad_shared,
        shared_norms,
    )


def solution(mesh):
    return jax.shard_map(
        on_device,
        mesh=mesh,
        in_specs=(
            P("ep", "tp"),
            P("ep", None),
            P("ep", None),
            P("ep", "tp"),
            P("ep", "tp", None),
            P("ep", "tp", None),
            P("ep", "tp", None),
            P("ep", None),
        ),
        out_specs=(
            P("ep", "tp"),
            P("ep", None),
            P("ep", "tp", None),
            P("ep", "tp", None),
            P("ep", "tp", None),
            P(None, "ep", "tp"),
            P("tp", "ep"),
            P("tp"),
        ),
        check_vma=False,
    )
```

profile of v0, /device:TPU:0, one launch (start us, length us, event | category | flops | bytes accessed | tf_op | source)
XLA Modules:
  0.0 189.0 jit_solution(876428887451017277)
XLA Ops:
  8.0 0.8 broadcast_multiply_fusion
  8.8 0.8 copy.30
  11.1 1.4 scatter_custom_fusion.1
  12.5 1.5 scatter_custom_fusion
  14.1 1.2 mul.83
  16.1 2.1 %gather_fusion.1 = bf16[320,768]{1,0:T(8,128)(2,1)S(1)} fusion(bf16[128,768]{1,0:T(8,128)(2,1)S(1)} %copy-done.1, s32[1024]{0:T(1024)S(1)} %get-tuple-element.45), kind=kCustom, calls=%fused_computation.1 | custom fusion | bytes 984320 | tf_op jit(solution)/shard_map/gather | solution.py:42
  18.4 2.1 %gather_fusion = bf16[320,768]{1,0:T(8,128)(2,1)S(1)} fusion(bf16[256,768]{1,0:T(8,128)(2,1)S(1)} %multiply_convert_fusion, s32[1024]{0:T(1024)S(1)} %get-tuple-element.46), kind=kCustom, calls=%fused_computation | custom fusion | bytes 984320 | tf_op jit(solution)/shard_map/gather | solution.py:43
  20.5 0.9 broadcast_select_fusion
  21.4 20.8 %all_to_all.17 = bf16[8,40,768]{2,1,0:T(8,128)(2,1)S(1)} all-to-all(bf16[8,40,768]{2,1,0:T(8,128)(2,1)S(1)} %get-tuple-element.37), channel_id=1, replica_groups=mesh['ep'=8,'tp'=4] {'ep'}, dimensions={0} | all-to-all | bytes 983040 | tf_op jit(solution)/shard_map/all_to_all | solution.py:47
  42.2 3.5 %all-to-all-start = ((bf16[8,40,768]{2,1,0:T(8,128)(2,1)}), bf16[8,40,768]{2,1,0:T(8,128)(2,1)S(1)}, u32[]{:S(2)}, u32[]{:S(2)}) async-start(bf16[8,40,768]{2,1,0:T(8,128)(2,1)} %get-tuple-element.38), calls=%async_computation | async-start | bytes 983040 | tf_op jit(solution)/shard_map/all_to_all | solution.py:48
  45.7 2.8 %fusion.28 = bf16[1,320,896]{2,1,0:T(8,128)(2,1)} fusion(bf16[320,768]{1,0:T(8,128)(2,1)S(1)} %bitcast.94, bf16[1,768,896]{2,1,0:T(8,128)(2,1)} %param.13), kind=kOutput, calls=%fused_computation.32 | convolution fusion | flops 440688640 | bytes 2441216 | tf_op jit(solution)/shard_map/erd,edf->erf/dot_general | solution.py:51
  48.6 1.5 fusion.25
  50.1 10.2 %all-to-all-done = bf16[8,40,768]{2,1,0:T(8,128)(2,1)S(1)} async-done(((bf16[8,40,768]{2,1,0:T(8,128)(2,1)}), bf16[8,40,768]{2,1,0:T(8,128)(2,1)S(1)}, u32[]{:S(2)}, u32[]{:S(2)}) %all-to-all-start) | async-done | bytes 491552 | tf_op jit(solution)/shard_map/all_to_all | solution.py:48
  60.2 3.0 %fusion.31 = bf16[1,320,896]{2,1,0:T(8,128)(2,1)} fusion(bf16[320,768]{1,0:T(8,128)(2,1)S(1)} %bitcast.98, bf16[1,768,896]{2,1,0:T(8,128)(2,1)} %param.14), kind=kOutput, calls=%fused_computation.33 | convolution fusion | flops 440688640 | bytes 2441216 | tf_op jit(solution)/shard_map/erd,edf->erf/dot_general | solution.py:52
  63.3 0.8 copy-done.2
  64.2 1.4 fusion.68
  65.7 60.3 %all-reduce.3.cloned.1.call-done = (bf16[1,320,896]{2,1,0:T(8,128)(2,1)}, bf16[1,320,896]{2,1,0:T(8,128)(2,1)}, bf16[1,320,896]{2,1,0:T(8,128)(2,1)}) async-done(((bf16[1,320,896]{2,1,0:T(8,128)(2,1)}, bf16[1,320,896]{2,1,0:T(8,128)(2,1)}, bf16[1,320,896]{2,1,0:T(8,128)(2,1)}), (bf16[1,320,896]{2,1,0:T(8,128)(2,1)}, bf16[1,320,896]{2,1,0:T(8,128)(2,1)}, ...) | async-done | bytes 1720336 | tf_op jit(solution)/shard_map/psum | solution.py:56
  125.9 2.0 %fusion.41 = bf16[320]{0:T(512)(128)(2,1)S(1)} fusion(bf16[1,320,896]{2,1,0:T(8,128)(2,1)} %get-tuple-element.32, bf16[1,320,896]{2,1,0:T(8,128)(2,1)} %get-tuple-element.33, bf16[1,320,896]{2,1,0:T(8,128)(2,1)} %get-tuple-element.34), kind=kLoop, calls=%fused_computation.39 | loop fusion | flops 2866880 | bytes 1720960 | tf_op jit(solution)/shard_map/reduce_sum | solution.py:19
  128.7 4.6 %all-to-all-start.3 = ((bf16[1,8,40]{2,0,1:T(2,128)(2,1)}), bf16[1,8,40]{2,0,1:T(2,128)(2,1)S(1)}, u32[]{:S(2)}, u32[]{:S(2)}) async-start(bf16[1,8,40]{2,0,1:T(2,128)(2,1)} %convert_element_type.103), calls=%async_computation.3 | async-start | bytes 8192 | tf_op jit(solution)/shard_map/all_to_all | solution.py:70
  133.3 1.0 fusion
  134.7 0.9 fusion.34
  135.7 2.6 %multiply_reduce_fusion = (f32[768]{0:T(1024)S(1)}, f32[768,896]{1,0:T(8,128)}) fusion(bf16[320,768]{1,0:T(8,128)(2,1)S(1)} %bitcast.99, bf16[1,320,896]{2,1,0:T(8,128)(2,1)S(1)} %copy-done.5, bf16[1,320,896]{2,1,0:T(8,128)(2,1)S(1)} %copy-done.7), kind=kOutput, calls=%fused_computation.6 | convolution fusion | flops 444071168 | bytes 4393984 | tf_op jit(solution)/shard_map/erd,erf->edf/dot_general | solution.py:63
  139.6 3.7 %reduce.11 = bf16[320,768]{1,0:T(8,128)(2,1)S(1)} reduce(bf16[320,1,768]{2,1,0:T(2,128)(2,1)S(1)} %bitcast.90, bf16[]{:T(256)} %broadcast.119), dimensions={1}, to_apply=%bitcast.88.reduce_sub_computation | reduce | bytes 983042
  143.3 0.9 reshape.256
  144.2 5.1 %all-to-all-start.2 = ((bf16[8,2,15360]{2,1,0:T(2,128)(2,1)}), bf16[8,2,15360]{2,1,0:T(2,128)(2,1)S(1)}, u32[]{:S(2)}, u32[]{:S(2)}) async-start(bf16[8,2,15360]{2,1,0:T(2,128)(2,1)} %reshape.256), calls=%async_computation.2 | async-start | bytes 983040 | tf_op jit(solution)/shard_map/all_to_all | solution.py:69
  149.4 3.8 %multiply_reduce_fusion.1 = (f32[768]{0:T(1024)S(1)}, f32[768,896]{1,0:T(8,128)}) fusion(bf16[320,768]{1,0:T(8,128)(2,1)S(1)} %bitcast.96, bf16[1,320,896]{2,1,0:T(8,128)(2,1)S(1)} %copy-done.4, bf16[1,320,896]{2,1,0:T(8,128)(2,1)} %get-tuple-element.34), kind=kOutput, calls=%fused_computation.7 | convolution fusion | flops 444071168 | bytes 4393984 | tf_op jit(solution)/shard_map/erd,erf->edf/dot_general | solution.py:62
  153.2 2.7 %multiply_reduce_fusion.2 = (f32[768]{0:T(1024)S(1)}, f32[768,896]{1,0:T(8,128)}) fusion(bf16[320,768]{1,0:T(8,128)(2,1)S(1)} %bitcast.97, bf16[1,320,896]{2,1,0:T(8,128)(2,1)S(1)} %copy-done.8, bf16[1,320,896]{2,1,0:T(8,128)(2,1)S(1)} %copy-done.6, bf16[1,320,896]{2,1,0:T(8,128)(2,1)S(1)} %copy-done.4), kind=kOutput, calls=%fused_computation.8 | convolution fusion | flops 445504768 | bytes 4967424 | tf_op jit(solution)/shard_map/erd,erf->edf/dot_general | solution.py:59
  156.6 1.9 %gather_fusion.3 = bf16[256]{0:T(256)(128)(2,1)S(1)} fusion(bf16[320]{0:T(512)(128)(2,1)S(1)} %reshape.197, s32[1024]{0:T(1024)S(1)} %pad_clamp_fusion), kind=kCustom, calls=%fused_computation.3 | custom fusion | bytes 2048 | tf_op jit(solution)/shard_map/gather | solution.py:75
  159.4 0.9 multiply_reduce_fusion.3
  160.3 17.7 %psum.31 = f32[768]{0:T(1024)} all-reduce(f32[768]{0:T(1024)S(1)} %multiply_reduce_fusion.3), channel_id=1, replica_groups=mesh['ep'=8,'tp'=4] {'ep'}, use_global_device_ids=true, to_apply=%region_15.16 | all-reduce | flops 768 | bytes 6144 | tf_op jit(solution)/shard_map/psum | solution.py:89
  178.5 1.2 gather_fusion.2
  179.8 1.7 reduce_sum.70
  (74 shorter events, 7.3 us)
Async XLA Ops:
  8.0 40.6 %copy-start = (bf16[1,768,896]{2,1,0:T(8,128)(2,1)S(1)}, bf16[1,768,896]{2,1,0:T(8,128)(2,1)}, u32[]{:S(2)}) copy-start(bf16[1,768,896]{2,1,0:T(8,128)(2,1)} %param.12) | copy-start | bytes 4128772
  14.1 1.7 copy-start.14
  14.1 2.0 %copy-start.1 = (bf16[128,768]{1,0:T(8,128)(2,1)S(1)}, bf16[128,768]{1,0:T(8,128)(2,1)}, u32[]{:S(2)}) copy-start(bf16[128,768]{1,0:T(8,128)(2,1)} %param.8) | copy-start | bytes 589828
  42.2 6.4 %copy-start.9 = (bf16[8,40,768]{2,1,0:T(8,128)(2,1)}, bf16[8,40,768]{2,1,0:T(8,128)(2,1)S(1)}, u32[]{:S(2)}) copy-start(bf16[8,40,768]{2,1,0:T(8,128)(2,1)S(1)} %all_to_all.17) | copy-start | bytes 1474564
  42.2 18.0 %all-to-all-start = ((bf16[8,40,768]{2,1,0:T(8,128)(2,1)}), bf16[8,40,768]{2,1,0:T(8,128)(2,1)S(1)}, u32[]{:S(2)}, u32[]{:S(2)}) async-start(bf16[8,40,768]{2,1,0:T(8,128)(2,1)} %get-tuple-element.38), calls=%async_computation | async-start | bytes 983040 | tf_op jit(solution)/shard_map/all_to_all | solution.py:48
  45.7 80.2 %all-reduce.3.cloned.1.call-start = ((), (), s32[]{:S(2)}) async-start(), calls=%async_computation.6 | async-start | bytes 3440640 | tf_op jit(solution)/shard_map/psum | solution.py:56
  60.2 3.0 %copy-start.11 = (bf16[8,40,768]{2,1,0:T(8,128)(2,1)}, bf16[8,40,768]{2,1,0:T(8,128)(2,1)S(1)}, u32[]{:S(2)}) copy-start(bf16[8,40,768]{2,1,0:T(8,128)(2,1)S(1)} %all-to-all-done) | copy-start | bytes 1474564
  63.3 0.9 copy-start.2
  63.3 1.0 copy-start.13
  63.3 96.1 %reduce-scatter.2.cloned.1.call-start = ((), (), s32[]{:S(2)}) async-start(), calls=%async_computation.5 | async-start | bytes 1548288 | tf_op jit(solution)/shard_map/reduce_scatter | solution.py:88
  125.9 7.3 %copy-start.3 = (bf16[1,320,896]{2,1,0:T(8,128)(2,1)S(1)}, bf16[1,320,896]{2,1,0:T(8,128)(2,1)}, u32[]{:S(2)}) copy-start(bf16[1,320,896]{2,1,0:T(8,128)(2,1)} %get-tuple-element.32) | copy-start | bytes 1720324
  125.9 7.3 %copy-start.5 = (bf16[1,320,896]{2,1,0:T(8,128)(2,1)S(1)}, bf16[1,320,896]{2,1,0:T(8,128)(2,1)}, u32[]{:S(2)}) copy-start(bf16[1,320,896]{2,1,0:T(8,128)(2,1)} %get-tuple-element.33) | copy-start | bytes 1720324
  125.9 7.4 %copy-start.7 = (bf16[1,320,896]{2,1,0:T(8,128)(2,1)S(1)}, bf16[1,320,896]{2,1,0:T(8,128)(2,1)}, u32[]{:S(2)}) copy-start(bf16[1,320,896]{2,1,0:T(8,128)(2,1)} %get-tuple-element.34) | copy-start | bytes 1720324
  128.7 15.6 %all-to-all-start.3 = ((bf16[1,8,40]{2,0,1:T(2,128)(2,1)}), bf16[1,8,40]{2,0,1:T(2,128)(2,1)S(1)}, u32[]{:S(2)}, u32[]{:S(2)}) async-start(bf16[1,8,40]{2,0,1:T(2,128)(2,1)} %convert_element_type.103), calls=%async_computation.3 | async-start | bytes 8192 | tf_op jit(solution)/shard_map/all_to_all | solution.py:70
  133.3 1.3 copy-start.15
  134.7 1.0 copy-start.12
  143.3 6.0 %copy-start.4 = (bf16[1,320,896]{2,1,0:T(8,128)(2,1)S(1)}, bf16[1,320,896]{2,1,0:T(8,128)(2,1)}, u32[]{:S(2)}) copy-start(bf16[1,320,896]{2,1,0:T(8,128)(2,1)} %get-tuple-element.32) | copy-start | bytes 1720324
  143.3 6.0 %copy-start.10 = (bf16[8,40,768]{2,1,0:T(8,128)(2,1)S(1)}, bf16[8,40,768]{2,1,0:T(8,128)(2,1)}, u32[]{:S(2)}) copy-start(bf16[8,40,768]{2,1,0:T(8,128)(2,1)} %copy-done.9) | copy-start | bytes 1474564
  144.2 33.8 %all-to-all-start.2 = ((bf16[8,2,15360]{2,1,0:T(2,128)(2,1)}), bf16[8,2,15360]{2,1,0:T(2,128)(2,1)S(1)}, u32[]{:S(2)}, u32[]{:S(2)}) async-start(bf16[8,2,15360]{2,1,0:T(2,128)(2,1)} %reshape.256), calls=%async_computation.2 | async-start | bytes 983040 | tf_op jit(solution)/shard_map/all_to_all | solution.py:69
  149.4 3.8 %copy-start.6 = (bf16[1,320,896]{2,1,0:T(8,128)(2,1)S(1)}, bf16[1,320,896]{2,1,0:T(8,128)(2,1)}, u32[]{:S(2)}) copy-start(bf16[1,320,896]{2,1,0:T(8,128)(2,1)} %get-tuple-element.33) | copy-start | bytes 1720324
  149.4 3.8 %copy-start.8 = (bf16[1,320,896]{2,1,0:T(8,128)(2,1)S(1)}, bf16[1,320,896]{2,1,0:T(8,128)(2,1)}, u32[]{:S(2)}) copy-start(bf16[1,320,896]{2,1,0:T(8,128)(2,1)} %get-tuple-element.34) | copy-start | bytes 1720324
Sparse Core Ops, SparseCore 0:
  63.4 62.4 all-reduce.2
Sparse Core Ops, SparseCore 1:
  66.6 32.3 reduce-scatter.1
where the time goes:
time: 190 us; the launch traced here: 189 us
  waiting for transfers between devices  70.5 us (37%)
  blocking collectives  38.5 us (20%)
  matrix products  19.8 us (10%)
  local copies, waits for them, and re-layouts  19.6 us (10%)
  between operations  15.8 us (8%)
  starting transfers between devices  13.3 us (7%)
  other arithmetic  11.7 us (6%)
    psum x1, waiting for transfers between devices, on_device(): lax.psum(down_part.astype(jnp.bfloat16), 'tp').astype(jnp.float32)  60.3 us
    all_to_all x1, blocking collectives, on_device(): lax.all_to_all(token_rows, 'ep', split_axis=0, concat_axis=1, tiled=True)  20.8 us
    psum x1, blocking collectives, on_device(): shared_norms = lax.psum(jnp.sum(grad_shared * grad_shared, axis=1), 'ep')  17.7 us
    all_to_all x1, waiting for transfers between devices, on_device(): lax.all_to_all(grad_rows, 'ep', split_axis=0, concat_axis=1, tiled=True)  10.2 us
    all_to_all x1, starting transfers between devices, on_device(): lax.all_to_all(token_back, 'ep', split_axis=1, concat_axis=0, tiled=True)  5.09 us
    unnamed x39, local copies, waits for them, and re-layouts  4.82 us
    all_to_all x1, starting transfers between devices, on_device(): lax.all_to_all(product, 'ep', split_axis=1, concat_axis=0, tiled=True)  4.61 us
  transfers between devices with their start and end apart: 5, of which 2 were waited for; matrix products, arithmetic and copies ran while one was open for 16% of the time, Pallas kernels for 0%

commit v1 on v0

--- a/solution.py
+++ b/solution.py
@@ -2,6 +2,13 @@
 import jax.numpy as jnp
 from jax import lax
 from jax.sharding import PartitionSpec as P
+
+
+def swap_blocks(array, axis, split, join):
+    n_dev = lax.axis_size(axis)
+    parts = jnp.stack(jnp.split(array, n_dev, axis=split), axis=0)
+    parts = lax.all_to_all(parts, axis, split_axis=0, concat_axis=0)
+    return jnp.concatenate(parts, axis=join)
 
 
 def slot_targets(routes, experts, capacity):
@@ -45,7 +52,7 @@
     grad_rows = grad_rows.reshape(experts, capacity, width_part)
     arrived_tok, arrived_grad = (
         lax.all_to_all(token_rows, "ep", split_axis=0, concat_axis=1, tiled=True),
-        lax.all_to_all(grad_rows, "ep", split_axis=0, concat_axis=1, tiled=True),
+        swap_blocks(grad_rows, "ep", 0, 1),
     )
     gate_part = jnp.einsum("erd,edf->erf", arrived_tok, w_gate, preferred_element_type=jnp.float32)
     up_part = jnp.einsum("erd,edf->erf", arrived_tok, w_up, preferred_element_type=jnp.float32)

time: 190 us -> 187 us (0.984)
  blocking collectives: 38.5 us -> 17.7 us
  starting transfers between devices: 13.3 us -> 19.6 us
  local copies, waits for them, and re-layouts: 19.6 us -> 24.2 us
  waiting for transfers between devices: 70.5 us -> 75 us
  matrix products: 19.8 us -> 21.9 us
    all_to_all x1 -> x0, blocking collectives: 20.8 us -> none  [on_device(): lax.all_to_all(token_rows, 'ep', split_axis=0, concat_axis=1, tiled=True)]
    all_to_all x1 -> x2, starting transfers between devices: 3.48 us -> 9.84 us  [the longest x1 6.35 us: on_device(): lax.all_to_all(token_rows, 'ep', split_axis=0, concat_axis=1, tiled=True)]
    unnamed x39 -> x44, local copies, waits for them, and re-layouts: 4.82 us -> 9.74 us
    all_to_all x1 -> x2, waiting for transfers between devices: 10.2 us -> 14.7 us  [the longest x1 9 us: swap_blocks(): parts = lax.all_to_all(parts, axis, split_axis=0, concat_axis=0)]
  transfers between devices with their start and end apart: 5 -> 6, of which waited for: 2 -> 3; matrix products, arithmetic and copies ran while one was open for 16% -> 22% of each run, Pallas kernels for 0% -> 0%
where the time goes in v1:
time: 187 us; the launch traced here: 186 us
  waiting for transfers between devices  75 us (40%)
  local copies, waits for them, and re-layouts  24.2 us (13%)
  matrix products  21.9 us (12%)
  starting transfers between devices  19.6 us (10%)
  blocking collectives  17.7 us (9%)
  between operations  15.8 us (8%)
  other arithmetic  11.8 us (6%)
    psum x1, waiting for transfers between devices, on_device(): lax.psum(down_part.astype(jnp.bfloat16), 'tp').astype(jnp.float32)  60.3 us
    psum x1, blocking collectives, on_device(): shared_norms = lax.psum(jnp.sum(grad_shared * grad_shared, axis=1), 'ep')  17.7 us
    unnamed x44, local copies, waits for them, and re-layouts  9.74 us
    all_to_all x1, waiting for transfers between devices, swap_blocks(): parts = lax.all_to_all(parts, axis, split_axis=0, concat_axis=0)  9 us
    all_to_all x1, starting transfers between devices, on_device(): lax.all_to_all(token_rows, 'ep', split_axis=0, concat_axis=1, tiled=True)  6.35 us
    all_to_all x1, waiting for transfers between devices, on_device(): lax.all_to_all(token_rows, 'ep', split_axis=0, concat_axis=1, tiled=True)  5.66 us
    all_to_all x1, starting transfers between devices, on_device(): lax.all_to_all(token_back, 'ep', split_axis=1, concat_axis=0, tiled=True)  5.09 us
    all_to_all x1, starting transfers between devices, on_device(): lax.all_to_all(product, 'ep', split_axis=1, concat_axis=0, tiled=True)  4.61 us
  transfers between devices with their start and end apart: 6, of which 3 were waited for; matrix products, arithmetic and copies ran while one was open for 22% of the time, Pallas kernels for 0%

profile of v1, /device:TPU:0, one launch (start us, length us, event | category | flops | bytes accessed | tf_op | source)
XLA Modules:
  0.0 186.1 jit_solution(642323159309392584)
XLA Ops:
  8.0 0.8 broadcast_multiply_fusion
  8.8 0.8 copy.30
  11.1 1.4 scatter_custom_fusion.1
  12.6 1.5 scatter_custom_fusion
  14.2 2.1 %gather_fusion.1 = bf16[320,768]{1,0:T(8,128)(2,1)S(1)} fusion(bf16[128,768]{1,0:T(8,128)(2,1)S(1)} %copy-done.1, s32[1024]{0:T(1024)S(1)} %get-tuple-element.43), kind=kCustom, calls=%fused_computation.1 | custom fusion | bytes 984320 | tf_op jit(solution)/shard_map/gather | solution.py:49
  16.3 0.9 broadcast_select_fusion.1
  17.2 6.4 %all-to-all-start.1 = ((bf16[8,40,768]{2,1,0:T(8,128)(2,1)}), bf16[8,40,768]{2,1,0:T(8,128)(2,1)}, u32[]{:S(2)}, u32[]{:S(2)}) async-start(bf16[8,40,768]{2,1,0:T(8,128)(2,1)} %broadcast_select_fusion.1), calls=%async_computation.1 | async-start | bytes 983040 | tf_op jit(solution)/shard_map/all_to_all | solution.py:54
  25.3 2.1 %gather_fusion = bf16[320,768]{1,0:T(8,128)(2,1)S(1)} fusion(bf16[256,768]{1,0:T(8,128)(2,1)S(1)} %multiply_convert_fusion, s32[1024]{0:T(1024)S(1)} %get-tuple-element.44), kind=kCustom, calls=%fused_computation | custom fusion | bytes 984320 | tf_op jit(solution)/shard_map/gather | solution.py:50
  32.6 5.7 %all-to-all-done.1 = bf16[8,40,768]{2,1,0:T(8,128)(2,1)} async-done(((bf16[8,40,768]{2,1,0:T(8,128)(2,1)}), bf16[8,40,768]{2,1,0:T(8,128)(2,1)}, u32[]{:S(2)}, u32[]{:S(2)}) %all-to-all-start.1) | async-done | bytes 491552 | tf_op jit(solution)/shard_map/all_to_all | solution.py:54
  38.3 3.5 %all-to-all-start = ((bf16[8,1,40,768]{3,2,1,0:T(8,128)(2,1)}), bf16[8,1,40,768]{3,2,1,0:T(8,128)(2,1)S(1)}, u32[]{:S(2)}, u32[]{:S(2)}) async-start(bf16[8,1,40,768]{3,2,1,0:T(8,128)(2,1)} %fusion.54), calls=%async_computation | async-start | bytes 983040 | tf_op jit(solution)/shard_map/all_to_all | solution.py:10
  41.8 3.0 %fusion.28 = bf16[1,320,896]{2,1,0:T(8,128)(2,1)} fusion(bf16[320,768]{1,0:T(8,128)(2,1)} %bitcast.16, bf16[1,768,896]{2,1,0:T(8,128)(2,1)} %param.13), kind=kOutput, calls=%fused_computation.32 | convolution fusion | flops 440688640 | bytes 2441216 | tf_op jit(solution)/shard_map/erd,edf->erf/dot_general | solution.py:58
  44.8 2.5 %fusion.25 = bf16[1,320,896]{2,1,0:T(8,128)(2,1)} fusion(bf16[320,768]{1,0:T(8,128)(2,1)} %bitcast.16, bf16[1,768,896]{2,1,0:T(8,128)(2,1)S(1)} %copy-done), kind=kOutput, calls=%fused_computation.31 | convolution fusion | flops 440688640 | bytes 2441216 | tf_op jit(solution)/shard_map/erd,edf->erf/dot_general | solution.py:57
  47.3 9.0 %all-to-all-done = bf16[8,1,40,768]{3,2,1,0:T(8,128)(2,1)S(1)} async-done(((bf16[8,1,40,768]{3,2,1,0:T(8,128)(2,1)}), bf16[8,1,40,768]{3,2,1,0:T(8,128)(2,1)S(1)}, u32[]{:S(2)}, u32[]{:S(2)}) %all-to-all-start) | async-done | bytes 491552 | tf_op jit(solution)/shard_map/all_to_all | solution.py:10
  56.3 3.0 %fusion.31 = bf16[1,320,896]{2,1,0:T(8,128)(2,1)} fusion(bf16[320,768]{1,0:T(8,128)(2,1)S(1)} %bitcast.124, bf16[1,768,896]{2,1,0:T(8,128)(2,1)} %param.14), kind=kOutput, calls=%fused_computation.33 | convolution fusion | flops 440688640 | bytes 2441216 | tf_op jit(solution)/shard_map/erd,edf->erf/dot_general | solution.py:59
  59.4 0.8 copy-done.12
  60.2 1.4 fusion.76
  61.7 60.3 %all-reduce.3.cloned.1.call-done = (bf16[1,320,896]{2,1,0:T(8,128)(2,1)}, bf16[1,320,896]{2,1,0:T(8,128)(2,1)}, bf16[1,320,896]{2,1,0:T(8,128)(2,1)}) async-done(((bf16[1,320,896]{2,1,0:T(8,128)(2,1)}, bf16[1,320,896]{2,1,0:T(8,128)(2,1)}, bf16[1,320,896]{2,1,0:T(8,128)(2,1)}), (bf16[1,320,896]{2,1,0:T(8,128)(2,1)}, bf16[1,320,896]{2,1,0:T(8,128)(2,1)}, ...) | async-done | bytes 1720336 | tf_op jit(solution)/shard_map/psum | solution.py:63
  122.0 2.0 %fusion.41 = bf16[320]{0:T(512)(128)(2,1)S(1)} fusion(bf16[1,320,896]{2,1,0:T(8,128)(2,1)} %get-tuple-element.32, bf16[1,320,896]{2,1,0:T(8,128)(2,1)} %get-tuple-element.33, bf16[1,320,896]{2,1,0:T(8,128)(2,1)} %get-tuple-element.34), kind=kLoop, calls=%fused_computation.39 | loop fusion | flops 2866880 | bytes 1720960 | tf_op jit(solution)/shard_map/reduce_sum | solution.py:26
  124.8 4.6 %all-to-all-start.3 = ((bf16[1,8,40]{2,0,1:T(2,128)(2,1)}), bf16[1,8,40]{2,0,1:T(2,128)(2,1)S(1)}, u32[]{:S(2)}, u32[]{:S(2)}) async-start(bf16[1,8,40]{2,0,1:T(2,128)(2,1)} %convert_element_type.103), calls=%async_computation.3 | async-start | bytes 8192 | tf_op jit(solution)/shard_map/all_to_all | solution.py:77
  129.4 1.0 fusion
  130.7 0.9 fusion.34
  131.8 2.6 %multiply_reduce_fusion = (f32[768]{0:T(1024)S(1)}, f32[768,896]{1,0:T(8,128)}) fusion(bf16[320,768]{1,0:T(8,128)(2,1)S(1)} %bitcast.125, bf16[1,320,896]{2,1,0:T(8,128)(2,1)S(1)} %copy-done.7, bf16[1,320,896]{2,1,0:T(8,128)(2,1)S(1)} %copy-done.9), kind=kOutput, calls=%fused_computation.6 | convolution fusion | flops 444071168 | bytes 4393984 | tf_op jit(solution)/shard_map/erd,erf->edf/dot_general | solution.py:70
  135.7 3.7 %reduce.11 = bf16[320,768]{1,0:T(8,128)(2,1)S(1)} reduce(bf16[320,1,768]{2,1,0:T(2,128)(2,1)S(1)} %bitcast.121, bf16[]{:T(256)} %broadcast.117), dimensions={1}, to_apply=%bitcast.119.reduce_sub_computation | reduce | bytes 983042
  139.4 0.9 reshape.264
  140.3 5.1 %all-to-all-start.2 = ((bf16[8,2,15360]{2,1,0:T(2,128)(2,1)}), bf16[8,2,15360]{2,1,0:T(2,128)(2,1)S(1)}, u32[]{:S(2)}, u32[]{:S(2)}) async-start(bf16[8,2,15360]{2,1,0:T(2,128)(2,1)} %reshape.264), calls=%async_computation.2 | async-start | bytes 983040 | tf_op jit(solution)/shard_map/all_to_all | solution.py:76
  145.4 3.7 %multiply_reduce_fusion.1 = (f32[768]{0:T(1024)S(1)}, f32[768,896]{1,0:T(8,128)}) fusion(bf16[320,768]{1,0:T(8,128)(2,1)} %bitcast.16, bf16[1,320,896]{2,1,0:T(8,128)(2,1)S(1)} %copy-done.6, bf16[1,320,896]{2,1,0:T(8,128)(2,1)S(1)} %copy-done.9), kind=kOutput, calls=%fused_computation.7 | convolution fusion | flops 444071168 | bytes 4393984 | tf_op jit(solution)/shard_map/erd,erf->edf/dot_general | solution.py:69
  149.1 3.8 %multiply_reduce_fusion.2 = (f32[768]{0:T(1024)S(1)}, f32[768,896]{1,0:T(8,128)}) fusion(bf16[320,768]{1,0:T(8,128)(2,1)} %bitcast.16, bf16[1,320,896]{2,1,0:T(8,128)(2,1)S(1)} %copy-done.9, bf16[1,320,896]{2,1,0:T(8,128)(2,1)S(1)} %copy-done.8, bf16[1,320,896]{2,1,0:T(8,128)(2,1)S(1)} %copy-done.6), kind=kOutput, calls=%fused_computation.8 | convolution fusion | flops 445504768 | bytes 4967424 | tf_op jit(solution)/shard_map/erd,erf->edf/dot_general | solution.py:66
  153.6 1.9 %gather_fusion.3 = bf16[256]{0:T(256)(128)(2,1)S(1)} fusion(bf16[320]{0:T(512)(128)(2,1)S(1)} %reshape.205, s32[1024]{0:T(1024)S(1)} %pad_clamp_fusion), kind=kCustom, calls=%fused_computation.3 | custom fusion | bytes 2048 | tf_op jit(solution)/shard_map/gather | solution.py:82
  156.4 0.9 multiply_reduce_fusion.3
  157.4 17.7 %psum.31 = f32[768]{0:T(1024)} all-reduce(f32[768]{0:T(1024)S(1)} %multiply_reduce_fusion.3), channel_id=1, replica_groups=mesh['ep'=8,'tp'=4] {'ep'}, use_global_device_ids=true, to_apply=%region_15.16 | all-reduce | flops 768 | bytes 6144 | tf_op jit(solution)/shard_map/psum | solution.py:96
  175.6 1.2 gather_fusion.2
  176.9 1.7 reduce_sum.70
  (82 shorter events, 13.2 us)
Async XLA Ops:
  8.0 36.8 %copy-start = (bf16[1,768,896]{2,1,0:T(8,128)(2,1)S(1)}, bf16[1,768,896]{2,1,0:T(8,128)(2,1)}, u32[]{:S(2)}) copy-start(bf16[1,768,896]{2,1,0:T(8,128)(2,1)} %param.12) | copy-start | bytes 4128772
  8.0 6.1 %copy-start.1 = (bf16[128,768]{1,0:T(8,128)(2,1)S(1)}, bf16[128,768]{1,0:T(8,128)(2,1)}, u32[]{:S(2)}) copy-start(bf16[128,768]{1,0:T(8,128)(2,1)} %param.8) | copy-start | bytes 589828
  16.3 7.3 %copy-start.2 = (bf16[128,768]{1,0:T(8,128)(2,1)S(1)}, bf16[128,768]{1,0:T(8,128)(2,1)}, u32[]{:S(2)}) copy-start(bf16[128,768]{1,0:T(8,128)(2,1)} %param.11) | copy-start | bytes 589828
  17.2 21.1 %all-to-all-start.1 = ((bf16[8,40,768]{2,1,0:T(8,128)(2,1)}), bf16[8,40,768]{2,1,0:T(8,128)(2,1)}, u32[]{:S(2)}, u32[]{:S(2)}) async-start(bf16[8,40,768]{2,1,0:T(8,128)(2,1)} %broadcast_select_fusion.1), calls=%async_computation.1 | async-start | bytes 983040 | tf_op jit(solution)/shard_map/all_to_all | solution.py:54
  23.6 0.8 copy-start.13
  24.5 0.6 copy-start.3
  38.3 18.0 %all-to-all-start = ((bf16[8,1,40,768]{3,2,1,0:T(8,128)(2,1)}), bf16[8,1,40,768]{3,2,1,0:T(8,128)(2,1)S(1)}, u32[]{:S(2)}, u32[]{:S(2)}) async-start(bf16[8,1,40,768]{3,2,1,0:T(8,128)(2,1)} %fusion.54), calls=%async_computation | async-start | bytes 983040 | tf_op jit(solution)/shard_map/all_to_all | solution.py:10
  41.8 80.2 %all-reduce.3.cloned.1.call-start = ((), (), s32[]{:S(2)}) async-start(), calls=%async_computation.6 | async-start | bytes 3440640 | tf_op jit(solution)/shard_map/psum | solution.py:63
  56.3 3.0 %copy-start.10 = (bf16[8,1,40,768]{3,2,1,0:T(8,128)(2,1)}, bf16[8,1,40,768]{3,2,1,0:T(8,128)(2,1)S(1)}, u32[]{:S(2)}) copy-start(bf16[8,1,40,768]{3,2,1,0:T(8,128)(2,1)S(1)} %all-to-all-done) | copy-start | bytes 1474564
  59.3 0.9 copy-start.12
  59.4 97.0 %reduce-scatter.2.cloned.1.call-start = ((), (), s32[]{:S(2)}) async-start(), calls=%async_computation.5 | async-start | bytes 1548288 | tf_op jit(solution)/shard_map/reduce_scatter | solution.py:95
  122.0 7.3 %copy-start.5 = (bf16[1,320,896]{2,1,0:T(8,128)(2,1)S(1)}, bf16[1,320,896]{2,1,0:T(8,128)(2,1)}, u32[]{:S(2)}) copy-start(bf16[1,320,896]{2,1,0:T(8,128)(2,1)} %get-tuple-element.32) | copy-start | bytes 1720324
  122.0 7.3 %copy-start.7 = (bf16[1,320,896]{2,1,0:T(8,128)(2,1)S(1)}, bf16[1,320,896]{2,1,0:T(8,128)(2,1)}, u32[]{:S(2)}) copy-start(bf16[1,320,896]{2,1,0:T(8,128)(2,1)} %get-tuple-element.33) | copy-start | bytes 1720324
  122.0 7.4 %copy-start.9 = (bf16[1,320,896]{2,1,0:T(8,128)(2,1)S(1)}, bf16[1,320,896]{2,1,0:T(8,128)(2,1)}, u32[]{:S(2)}) copy-start(bf16[1,320,896]{2,1,0:T(8,128)(2,1)} %get-tuple-element.34) | copy-start | bytes 1720324
  124.8 15.6 %all-to-all-start.3 = ((bf16[1,8,40]{2,0,1:T(2,128)(2,1)}), bf16[1,8,40]{2,0,1:T(2,128)(2,1)S(1)}, u32[]{:S(2)}, u32[]{:S(2)}) async-start(bf16[1,8,40]{2,0,1:T(2,128)(2,1)} %convert_element_type.103), calls=%async_computation.3 | async-start | bytes 8192 | tf_op jit(solution)/shard_map/all_to_all | solution.py:77
  129.4 1.3 copy-start.14
  130.7 1.0 copy-start.11
  139.4 6.0 %copy-start.6 = (bf16[1,320,896]{2,1,0:T(8,128)(2,1)S(1)}, bf16[1,320,896]{2,1,0:T(8,128)(2,1)}, u32[]{:S(2)}) copy-start(bf16[1,320,896]{2,1,0:T(8,128)(2,1)} %get-tuple-element.32) | copy-start | bytes 1720324
  140.3 34.8 %all-to-all-start.2 = ((bf16[8,2,15360]{2,1,0:T(2,128)(2,1)}), bf16[8,2,15360]{2,1,0:T(2,128)(2,1)S(1)}, u32[]{:S(2)}, u32[]{:S(2)}) async-start(bf16[8,2,15360]{2,1,0:T(2,128)(2,1)} %reshape.264), calls=%async_computation.2 | async-start | bytes 983040 | tf_op jit(solution)/shard_map/all_to_all | solution.py:76
  145.4 3.7 %copy-start.8 = (bf16[1,320,896]{2,1,0:T(8,128)(2,1)S(1)}, bf16[1,320,896]{2,1,0:T(8,128)(2,1)}, u32[]{:S(2)}) copy-start(bf16[1,320,896]{2,1,0:T(8,128)(2,1)} %get-tuple-element.33) | copy-start | bytes 1720324
  149.1 6.6 %copy-start.4 = (f32[128,2]{1,0:T(8,128)S(1)}, f32[128,2]{1,0:T(8,128)}, u32[]{:S(2)}) copy-start(f32[128,2]{1,0:T(8,128)} %copy-done.3) | copy-start | bytes 3076
Sparse Core Ops, SparseCore 0:
  59.5 62.4 all-reduce.2
Sparse Core Ops, SparseCore 1:
  62.7 32.3 reduce-scatter.1
